TPU v7x, 256 devices: a 4x2x16 block of a 4x16x16 slice. The times are simulated.
256 devices in a mesh: grp: 2 (over y), sp: 16 (over z), tp: 8 (over x, core).
Axes of the slice: x: 4, y: 2, z: 16, core: 2. Of those that a mesh axis runs over, the one named last changes fastest.
The devices are a block of a 4x16x16 slice.
Arguments:
- queries: bfloat16 [24576, 1024], P(('grp', 'sp'), 'tp'), parts along dimension 0, may hold values from -200 to 200
- key_rows: bfloat16 [24576, 512], P(('grp', 'sp'), 'tp'), parts along dimension 0, may hold values from -6 to 6
- value_rows: bfloat16 [24576, 512], P(('grp', 'sp'), 'tp'), parts along dimension 0, may hold values from -6 to 6
- doc_ids: int32 [24576], P(('grp', 'sp')), parts along dimension 0, may hold values from 0 to 7, never falling along the last dimension, each value on 1 to 3072 neighbouring positions
- sink_logits: float32 [16], P('tp'), may hold values from 2 to 7
- out_weight: bfloat16 [1024, 2048], P('tp', 'sp'), may hold values from -0.1875 to 0.1875
- residual: bfloat16 [24576, 2048], P(('grp', 'sp', 'tp')), parts along dimension 0, may hold values from -6 to 6
- gain_mixed: float32 [2048], replicated, may hold values from 0.1 to 1.9
- gain_before: float32 [2048], replicated, may hold values from 0.1 to 1.9
- gain_after: float32 [2048], replicated, may hold values from 0.1 to 1.9
- gate_weight: bfloat16 [2048, 6144], P('sp', 'tp'), may hold values from -0.125 to 0.125
- up_weight: bfloat16 [2048, 6144], P('sp', 'tp'), may hold values from -0.125 to 0.125
- down_weight: bfloat16 [6144, 2048], P('tp', 'sp'), may hold values from -0.078125 to 0.078125
Outputs:
- layer_out: bfloat16 [24576, 2048], P(('grp', 'sp', 'tp')), parts along dimension 0
There are 2 independent parts, one for each index of `grp`. A program takes and returns all parts, laid end to end along the dimension named above; an argument that names none is the same for every part. Nothing has to cross between parts.
All inputs are finite; a program needn't handle non-finite values.
Results may differ from a plain program's by a relative error of at most 0.015.
Values may be sent and summed in bfloat16 or wider, within the bound.
A program may use at most 128 MiB of HBM per device.

v0:
```python
import jax
import jax.numpy as jnp
from jax import lax
from jax.sharding import PartitionSpec as P

HEAD_DIM = 64
WINDOW = 128
epsilon = 1e-06
masked_value = -1e30


def passed_along(value, axis, steps):
    count = lax.axis_size(axis)
    first, last = (max(0, -steps), min(count, count - steps))
    return lax.ppermute(value, axis, [(source, source + steps) for source in range(first, last)])


def from_everyone(shard, axis):
    size = lax.axis_size(axis)
    return lax.all_to_all(
        jnp.broadcast_to(shard[None], (size, *shard.shape)), axis, 0, 0, tiled=True
    )


def laid_out(pieces, dim):
    pieces = jnp.moveaxis(pieces, 0, dim)
    lengths = pieces.shape
    return pieces.reshape(*lengths[:dim], lengths[dim] * lengths[dim + 1], *lengths[dim + 2 :])


def gather_directly(shard, axis, dim):
    pieces = from_everyone(shard, axis)
    return laid_out(pieces, dim)


def turned_gather(arrays, axis, dims):
    turned = [jnp.moveaxis(a, dim, 0) for a, dim in zip(arrays, dims)]
    both = jnp.concatenate([t.reshape(len(t), -1) for t in turned], axis=1)
    filled, at, finished = (lax.all_gather(both, axis, axis=0, tiled=True), 0, [])
    for t, dim in zip(turned, dims):
        piece = filled[:, at : at + t[0].size].reshape(-1, *t.shape[1:])
        finished.append(jnp.moveaxis(piece, 0, dim))
        at += t[0].size
    return tuple(finished)


def split_up(shard, dim, size):
    lengths = shard.shape
    pieces = shard.reshape(*lengths[:dim], size, lengths[dim] // size, *lengths[dim + 1 :])
    return jnp.moveaxis(pieces, dim, 0)


def summed_on_arrival(shard, axis, dim):
    size = lax.axis_size(axis)
    pieces = lax.all_to_all(split_up(shard, dim, size), axis, 0, 0, tiled=True)
    return jnp.sum(pieces.astype(jnp.float32), axis=0)


def stored(value):
    return lax.optimization_barrier(value.astype(jnp.bfloat16)).astype(jnp.float32)


def rms_scaled(value, gain):
    return value * lax.rsqrt(jnp.mean(value * value, axis=-1, keepdims=True) + epsilon) * gain


def windows(array, blocks):
    first = array[:-WINDOW].reshape((blocks, WINDOW) + array.shape[1:])
    second = array[WINDOW:].reshape((blocks, WINDOW) + array.shape[1:])
    return jnp.concatenate([first, second], axis=1)


def attend(queries, key_rows, value_rows, doc_ids, sink_logits):
    length = queries.shape[0]
    blocks = length // WINDOW
    local_kv = key_rows.shape[1] // HEAD_DIM
    group_size = queries.shape[1] // HEAD_DIM // local_kv
    offset = lax.axis_index("sp") * length
    tail_keys, tail_values, tail_docs = passed_along(
        (key_rows[length - WINDOW :], value_rows[length - WINDOW :], doc_ids[length - WINDOW :]),
        "sp",
        1,
    )
    key_blocks = windows(jnp.concatenate([tail_keys, key_rows], axis=0), blocks).reshape(
        blocks, 2 * WINDOW, local_kv, HEAD_DIM
    )
    value_blocks = windows(jnp.concatenate([tail_values, value_rows], axis=0), blocks).reshape(
        blocks, 2 * WINDOW, local_kv, HEAD_DIM
    )
    key_docs = windows(jnp.concatenate([tail_docs, doc_ids], axis=0), blocks)
    key_places = windows(offset - WINDOW + jnp.arange(length + WINDOW, dtype=jnp.int32), blocks)
    query_places = (offset + jnp.arange(length, dtype=jnp.int32)).reshape(blocks, WINDOW)
    query_docs = doc_ids.reshape(blocks, WINDOW)
    query_blocks = queries.reshape(blocks, WINDOW, local_kv, group_size, HEAD_DIM)
    scores = jnp.einsum(
        "bqhgd,bkhd->bhgqk", query_blocks, key_blocks, preferred_element_type=jnp.float32
    ) * HEAD_DIM ** (-0.5)
    distance = query_places[:, :, None] - key_places[:, None, :]
    valid = (distance >= 0) & (distance < WINDOW) & (key_places[:, None, :] >= 0)
    valid = valid & (query_docs[:, :, None] == key_docs[:, None, :])
    scores = jnp.where(valid[:, None, None], scores, masked_value)
    sinks = sink_logits.reshape(local_kv, group_size)[None, :, :, None]
    top = jnp.maximum(jnp.max(scores, axis=-1), sinks)
    weight = jnp.exp(scores - top[..., None])
    denom = jnp.sum(weight, axis=-1) + jnp.exp(sinks - top)
    summed = jnp.einsum(
        "bhgqk,bkhd->bqhgd",
        weight.astype(jnp.bfloat16),
        value_blocks,
        preferred_element_type=jnp.float32,
    )
    scale = jnp.transpose(denom, (0, 3, 1, 2))[..., None]
    return (summed / scale).reshape(length, queries.shape[1]).astype(jnp.bfloat16)


def per_device(
    queries,
    key_rows,
    value_rows,
    doc_ids,
    sink_logits,
    out_weight,
    residual,
    gain_mixed,
    gain_before,
    gain_after,
    gate_weight,
    up_weight,
    down_weight,
):
    mixed = attend(queries, key_rows, value_rows, doc_ids, sink_logits)
    head_columns = gather_directly(out_weight, "sp", 1)
    by_rows = lax.all_to_all(mixed, "tp", split_axis=0, concat_axis=1, tiled=True)
    projected = jnp.dot(
        by_rows,
        lax.all_gather(head_columns, "tp", axis=0, tiled=True),
        preferred_element_type=jnp.float32,
    )
    projected = stored(projected)
    after = stored(residual.astype(jnp.float32) + rms_scaled(projected, gain_mixed))
    normed = rms_scaled(after, gain_before).astype(jnp.bfloat16)
    full_gate, full_up, full_down = turned_gather(
        (gate_weight, up_weight, down_weight), "sp", (0, 0, 1)
    )
    piece = lax.all_gather(normed, "tp", axis=0, tiled=True)
    gate = jnp.dot(piece, full_gate, preferred_element_type=jnp.float32)
    upward = jnp.dot(piece, full_up, preferred_element_type=jnp.float32)
    hidden = (jax.nn.silu(gate) * upward).astype(jnp.bfloat16)
    ffn_out = stored(
        summed_on_arrival(
            jnp.dot(hidden, full_down, preferred_element_type=jnp.float32).astype(jnp.bfloat16),
            "tp",
            0,
        )
    )
    return (after + 0.5 * rms_scaled(ffn_out, gain_after)).astype(jnp.bfloat16)


def solution(mesh):
    return jax.shard_map(
        per_device,
        mesh=mesh,
        in_specs=(
            P(("grp", "sp"), "tp"),
            P(("grp", "sp"), "tp"),
            P(("grp", "sp"), "tp"),
            P(("grp", "sp")),
            P("tp"),
            P("tp", "sp"),
            P(("grp", "sp", "tp"), None),
            P(),
            P(),
            P(),
            P("sp", "tp"),
            P("sp", "tp"),
            P("tp", "sp"),
        ),
        out_specs=P(("grp", "sp", "tp"), None),
        check_vma=False,
    )
```

profile of v0, /device:TPU:33, one launch (start us, length us, event | category | flops | bytes accessed | tf_op | source)
XLA Modules:
  0.0 348.9 jit_solution(4281266326615611289)
XLA Ops:
  6.6 0.1 all-gather.4.cloned.1.call-start
  6.6 1.0 copy.40
  7.6 0.1 broadcast_in_dim.16
  7.7 47.2 %all_to_all.26 = bf16[16,128,128]{1,2,0:T(8,128)(2,1)} all-to-all(bf16[16,128,128]{1,2,0:T(8,128)(2,1)S(1)} %broadcast_in_dim.16), channel_id=1, replica_groups=mesh['grp'=2,'sp'=16,'tp'=8] {'sp'}, dimensions={0} | all-to-all | bytes 1048576 | tf_op jit(solution)/shard_map/all_to_all | solution.py:20
  54.9 0.1 all-gather.4.cloned.1.call-update
  54.9 0.1 all-gather.6.cloned.1.call-start
  55.0 0.7 slice.49
  55.7 5.3 %collective-permute-start.1 = (s32[128]{0:T(128)S(1)}, s32[128]{0:T(128)S(1)}, u32[]{:S(2)}, u32[]{:S(2)}) collective-permute-start(s32[128]{0:T(128)S(1)} %slice.49), channel_id=1, source_target_pairs={{0,8},{8,16},{16,24},{24,32},{32,40},{40,48},{48,56},{56,64},{64,7... | collective-permute-start | bytes 1544 | tf_op jit(solution)/shard_map/ppermute | solution.py:15
  61.0 0.7 slice.45
  61.7 2.2 collective-permute-start
  63.9 0.7 slice.52
  64.6 4.6 %collective-permute-start.2 = (bf16[128,64]{0,1:T(8,128)(2,1)S(1)}, bf16[128,64]{0,1:T(8,128)(2,1)S(1)}, u32[]{:S(2)}, u32[]{:S(2)}) collective-permute-start(bf16[128,64]{0,1:T(8,128)(2,1)S(1)} %slice.52), channel_id=1, source_target_pairs={{0,8},{8,16},{16,24},{24,32},{32,40},{40,48},{48,56},{56,64},{64,7... | collective-permute-start | bytes 49160 | tf_op jit(solution)/shard_map/ppermute | solution.py:15
  69.3 0.2 reshape.170
  69.5 0.0 collective-permute-done.1
  69.6 1.0 fusion.30
  70.6 0.0 collective-permute-done.2
  70.6 0.0 collective-permute-done
  70.6 0.5 fusion.48
  71.1 0.1 broadcast_maximum_fusion
  71.2 0.2 fusion.7
  71.4 0.1 fusion.43
  71.5 0.4 fusion.13
  71.9 0.4 copy.48
  72.3 0.2 reshape.171
  72.5 17.5 %all_to_all.27 = bf16[8,96,128]{2,1,0:T(8,128)(2,1)S(1)} all-to-all(bf16[8,96,128]{2,1,0:T(8,128)(2,1)S(1)} %reshape.171), channel_id=1, replica_groups=mesh['grp'=2,'sp'=16,'tp'=8] {'tp'}, dimensions={0} | all-to-all | bytes 393216 | tf_op jit(solution)/shard_map/all_to_all | solution.py:133
  90.0 12.1 %all-gather.4.cloned.1.call-done = bf16[1024,2048]{0,1:T(8,128)(2,1)} async-done(((bf16[128,2048]{0,1:T(8,128)(2,1)}), bf16[1024,2048]{0,1:T(8,128)(2,1)}) %all-gather.4.cloned.1.call-update) | async-done | bytes 4194320 | tf_op jit(solution)/shard_map/all_gather | solution.py:136
  102.2 3.6 %convolution_convert_fusion.1 = bf16[96,2048]{1,0:T(8,128)(2,1)S(1)} fusion(bf16[1024,2048]{0,1:T(8,128)(2,1)} %all-gather.4.cloned.1.call-done, bf16[8,96,128]{2,1,0:T(8,128)(2,1)S(1)} %all_to_all.27), kind=kOutput, calls=%fused_computation.7 | convolution fusion | flops 402849792 | bytes 4784128 | tf_op jit(solution)/shard_map/dot_general | solution.py:134
  105.8 0.0 copy-start.4
  105.8 0.0 copy-start.5
  105.8 0.0 copy-start.3
  105.8 0.2 fusion.14
  106.0 0.2 fusion.17
  106.2 0.2 fusion.21
  106.4 0.9 fusion.23
  107.3 0.1 all-gather.6.cloned.1.call-update
  107.4 0.2 all-gather.8.cloned.1.call-start
  107.6 0.2 copy.41
  107.8 0.2 copy.42
  108.0 0.9 pad_maximum_fusion
  108.9 0.1 all-gather.8.cloned.1.call-update
  108.9 31.3 %all-gather.6.cloned.1.call-done = bf16[768,2048]{1,0:T(8,128)(2,1)} async-done(((bf16[96,2048]{1,0:T(8,128)(2,1)}), bf16[768,2048]{1,0:T(8,128)(2,1)}) %all-gather.6.cloned.1.call-update) | async-done | bytes 3145744 | tf_op jit(solution)/shard_map/all_gather | solution.py:145
  140.2 128.3 %all-gather.8.cloned.1.call-done = bf16[2048,2304]{0,1:T(8,128)(2,1)} async-done(((bf16[128,2304]{0,1:T(8,128)(2,1)}), bf16[2048,2304]{0,1:T(8,128)(2,1)}) %all-gather.8.cloned.1.call-update) | async-done | bytes 9437200 | tf_op jit(solution)/shard_map/all_gather | solution.py:39
  268.5 6.9 %fusion.3 = f32[768,768]{1,0:T(8,128)} fusion(bf16[768,2048]{1,0:T(8,128)(2,1)} %all-gather.6.cloned.1.call-done, bf16[2048,2304]{0,1:T(8,128)(2,1)} %all-gather.8.cloned.1.call-done), kind=kOutput, calls=%fused_computation.4 | convolution fusion | flops 2415919104 | bytes 8650752 | tf_op jit(solution)/shard_map/dot_general | solution.py:146
  275.4 11.0 %convolution_convert_fusion = bf16[768,2048]{1,0:T(8,128)(2,1)} fusion(bf16[2048,2304]{0,1:T(8,128)(2,1)} %all-gather.8.cloned.1.call-done, f32[768,768]{1,0:T(8,128)} %fusion.3, bf16[768,2048]{1,0:T(8,128)(2,1)S(1)} %copy-done.12), kind=kOutput, calls=%fused_computation | convolution fusion | flops 4836950016 | bytes 14942208 | tf_op jit(solution)/shard_map/dot_general | solution.py:151
  286.4 51.4 %all_to_all.28 = bf16[8,96,2048]{2,1,0:T(8,128)(2,1)S(1)} all-to-all(bf16[8,96,2048]{2,1,0:T(8,128)(2,1)} %bitcast.84), channel_id=1, replica_groups=mesh['grp'=2,'sp'=16,'tp'=8] {'tp'}, dimensions={0} | all-to-all | bytes 6291456 | tf_op jit(solution)/shard_map/all_to_all | solution.py:55
  337.7 1.4 reduce_sum.54
  339.2 1.2 fusion.18
  340.4 2.0 fusion.24
  (37 shorter events, 0.2 us)
Async XLA Ops:
  6.5 63.0 %copy-start.7 = (s32[768]{0:T(1024)S(1)}, s32[768]{0:T(1024)}, u32[]{:S(2)}) copy-start(s32[768]{0:T(1024)} %param.16) | copy-start | bytes 9220
  6.5 62.7 %copy-start.1 = (bf16[768,64]{0,1:T(8,128)(2,1)S(1)}, bf16[768,64]{0,1:T(8,128)(2,1)}, u32[]{:S(2)}) copy-start(bf16[768,64]{0,1:T(8,128)(2,1)} %param.15) | copy-start | bytes 294916
  6.6 62.7 %copy-start = (bf16[768,64]{0,1:T(8,128)(2,1)S(1)}, bf16[768,64]{0,1:T(8,128)(2,1)}, u32[]{:S(2)}) copy-start(bf16[768,64]{0,1:T(8,128)(2,1)} %param.14) | copy-start | bytes 294916
  6.6 62.8 %copy-start.6 = (bf16[768,128]{1,0:T(8,128)(2,1)S(1)}, bf16[768,128]{1,0:T(8,128)(2,1)}, u32[]{:S(2)}) copy-start(bf16[768,128]{1,0:T(8,128)(2,1)} %param.13) | copy-start | bytes 589828
  6.6 95.6 %all-gather.4.cloned.1.call-start = ((), (), s32[]{:S(2)}) async-start(), calls=%async_computation.3 | async-start | bytes 4718592 | tf_op jit(solution)/shard_map/all_gather | solution.py:136
  54.9 16.2 %copy-start.11 = (f32[2]{0:T(128)S(1)}, f32[2]{0:T(128)}, u32[]{:S(2)}) copy-start(f32[2]{0:T(128)} %param.17) | copy-start | bytes 28
  54.9 85.2 %all-gather.6.cloned.1.call-start = ((), (), s32[]{:S(2)}) async-start(), calls=%async_computation.4 | async-start | bytes 3538944 | tf_op jit(solution)/shard_map/all_gather | solution.py:145
  55.7 13.8 %collective-permute-start.1 = (s32[128]{0:T(128)S(1)}, s32[128]{0:T(128)S(1)}, u32[]{:S(2)}, u32[]{:S(2)}) collective-permute-start(s32[128]{0:T(128)S(1)} %slice.49), channel_id=1, source_target_pairs={{0,8},{8,16},{16,24},{24,32},{32,40},{40,48},{48,56},{56,64},{64,7... | collective-permute-start | bytes 1544 | tf_op jit(solution)/shard_map/ppermute | solution.py:15
  61.7 8.9 %collective-permute-start = (bf16[128,64]{0,1:T(8,128)(2,1)S(1)}, bf16[128,64]{0,1:T(8,128)(2,1)S(1)}, u32[]{:S(2)}, u32[]{:S(2)}) collective-permute-start(bf16[128,64]{0,1:T(8,128)(2,1)S(1)} %slice.45), channel_id=1, source_target_pairs={{0,8},{8,16},{16,24},{24,32},{32,40},{40,48},{48,56},{56,64},{64,7... | collective-permute-start | bytes 49160 | tf_op jit(solution)/shard_map/ppermute | solution.py:15
  64.6 5.9 %collective-permute-start.2 = (bf16[128,64]{0,1:T(8,128)(2,1)S(1)}, bf16[128,64]{0,1:T(8,128)(2,1)S(1)}, u32[]{:S(2)}, u32[]{:S(2)}) collective-permute-start(bf16[128,64]{0,1:T(8,128)(2,1)S(1)} %slice.52), channel_id=1, source_target_pairs={{0,8},{8,16},{16,24},{24,32},{32,40},{40,48},{48,56},{56,64},{64,7... | collective-permute-start | bytes 49160 | tf_op jit(solution)/shard_map/ppermute | solution.py:15
  90.0 16.0 %copy-start.2 = (bf16[96,2048]{1,0:T(8,128)(2,1)S(1)}, bf16[96,2048]{1,0:T(8,128)(2,1)}, u32[]{:S(2)}) copy-start(bf16[96,2048]{1,0:T(8,128)(2,1)} %param.19) | copy-start | bytes 1179652
  90.0 16.0 %copy-start.8 = (f32[2048]{0:T(1024)S(1)}, f32[2048]{0:T(1024)}, u32[]{:S(2)}) copy-start(f32[2048]{0:T(1024)} %param.20) | copy-start | bytes 24580
  90.0 16.4 %copy-start.9 = (f32[2048]{0:T(1024)S(1)}, f32[2048]{0:T(1024)}, u32[]{:S(2)}) copy-start(f32[2048]{0:T(1024)} %param.21) | copy-start | bytes 24580
  105.8 1.9 copy-start.4
  105.8 2.0 copy-start.5
  105.8 2.2 copy-start.3
  107.4 161.1 %all-gather.8.cloned.1.call-start = ((), (), s32[]{:S(2)}) async-start(), calls=%async_computation.5 | async-start | bytes 10027008 | tf_op jit(solution)/shard_map/all_gather | solution.py:39
  140.2 135.2 %copy-start.12 = (bf16[768,2048]{1,0:T(8,128)(2,1)S(1)}, bf16[768,2048]{1,0:T(8,128)(2,1)}, u32[]{:S(2)}) copy-start(bf16[768,2048]{1,0:T(8,128)(2,1)} %all-gather.6.cloned.1.call-done) | copy-start | bytes 9437188
  337.7 2.6 copy-start.10
Sparse Core Ops, SparseCore 0:
  55.1 47.0 all-gather.3
  107.5 32.6 all-gather.5
  141.9 126.5 all-gather.7
where the time goes:
time: 349 us
  waiting for transfers between devices  172 us (49%)
  blocking collectives  116 us (33%)
  matrix products  22.3 us (6%)
  between operations  13.5 us (4%)
  starting transfers between devices  12.4 us (4%)
  other arithmetic  8.34 us (2%)
  local copies, waits for them, and re-layouts  4.39 us (1%)
    all_gather x1, waiting for transfers between devices, turned_gather(): lax.all_gather(both, axis, axis=0, tiled=True)  128 us
    all_to_all x1, blocking collectives, summed_on_arrival(): pieces = lax.all_to_all(split_up(shard, dim, size), axis, 0, 0, tiled=True)  51.4 us
    all_to_all x1, blocking collectives, from_everyone(): lax.all_to_all(jnp.broadcast_to(shard[None], (size, *shard.shape)), axis,...  47.2 us
    all_gather x1, waiting for transfers between devices, per_device(): piece = lax.all_gather(normed, 'tp', axis=0, tiled=True)  31.3 us
    all_to_all x1, blocking collectives, per_device(): lax.all_to_all(mixed, 'tp', split_axis=0, concat_axis=1, tiled=True)  17.5 us
    all_gather x1, waiting for transfers between devices, per_device(): lax.all_gather(head_columns, 'tp', axis=0, tiled=True)  12.1 us
    ppermute x3, starting transfers between devices, passed_along(): lax.ppermute(value, axis, [(source, source + steps) for source in range(f...  12 us
    dot_general x1, matrix products, per_device(): jnp.dot(hidden, full_down, preferred_element_type=jnp.float32)  11 us
  transfers between devices with their start and end apart: 6, of which 3 were waited for; matrix products, arithmetic and copies ran while one was open for 2% of the time, Pallas kernels for 0%

commit v1 on v0

--- a/solution.py
+++ b/solution.py
@@ -142,7 +142,11 @@
     full_gate, full_up, full_down = turned_gather(
         (gate_weight, up_weight, down_weight), "sp", (0, 0, 1)
     )
-    piece = lax.all_gather(normed, "tp", axis=0, tiled=True)
+    seen = []
+    for _ in range(lax.axis_size("tp")):
+        seen.append(normed)
+    arr_next = jnp.concatenate(seen, axis=0)
+    piece = lax.all_to_all(arr_next, "tp", 0, 0, tiled=True)
     gate = jnp.dot(piece, full_gate, preferred_element_type=jnp.float32)
     upward = jnp.dot(piece, full_up, preferred_element_type=jnp.float32)
     hidden = (jax.nn.silu(gate) * upward).astype(jnp.bfloat16)

time: 349 us -> 312 us (0.89)
  waiting for transfers between devices: 172 us -> 91.8 us
  blocking collectives: 116 us -> 158 us
    all_gather x1, waiting for transfers between devices: 128 us -> 82.2 us  [turned_gather(): lax.all_gather(both, axis, axis=0, tiled=True)]
    all_to_all x0 -> x1, blocking collectives: none -> 41.4 us  [per_device(): piece = lax.all_to_all(arr_next, 'tp', 0, 0, tiled=True)]
    all_gather x1 -> x0, waiting for transfers between devices: 31.3 us -> none  [per_device(): piece = lax.all_gather(normed, 'tp', axis=0, tiled=True)]
  transfers between devices with their start and end apart: 6 -> 5, of which waited for: 3 -> 2; matrix products, arithmetic and copies ran while one was open for 2% -> 4% of each run, Pallas kernels for 0% -> 0%
where the time goes in v1:
time: 312 us; the launch traced here: 311 us
  blocking collectives  158 us (51%)
  waiting for transfers between devices  91.8 us (29%)
  matrix products  21.4 us (7%)
  between operations  13.8 us (4%)
  starting transfers between devices  12.2 us (4%)
  other arithmetic  9.62 us (3%)
  local copies, waits for them, and re-layouts  4.12 us (1%)
    all_gather x1, waiting for transfers between devices, turned_gather(): lax.all_gather(both, axis, axis=0, tiled=True)  82.2 us
    all_to_all x1, blocking collectives, summed_on_arrival(): pieces = lax.all_to_all(split_up(shard, dim, size), axis, 0, 0, tiled=True)  51.4 us
    all_to_all x1, blocking collectives, from_everyone(): lax.all_to_all(jnp.broadcast_to(shard[None], (size, *shard.shape)), axis,...  47.2 us
    all_to_all x1, blocking collectives, per_device(): piece = lax.all_to_all(arr_next, 'tp', 0, 0, tiled=True)  41.4 us
    all_to_all x1, blocking collectives, per_device(): lax.all_to_all(mixed, 'tp', split_axis=0, concat_axis=1, tiled=True)  18 us
    ppermute x3, starting transfers between devices, passed_along(): lax.ppermute(value, axis, [(source, source + steps) for source in range(f...  12.1 us
    dot_general x1, matrix products, per_device(): jnp.dot(hidden, full_down, preferred_element_type=jnp.float32)  11 us
    all_gather x1, waiting for transfers between devices, per_device(): lax.all_gather(head_columns, 'tp', axis=0, tiled=True)  9.57 us
  transfers between devices with their start and end apart: 5, of which 2 were waited for; matrix products, arithmetic and copies ran while one was open for 4% of the time, Pallas kernels for 0%

profile of v1, /device:TPU:33, one launch (start us, length us, event | category | flops | bytes accessed | tf_op | source)
XLA Modules:
  0.0 310.9 jit_solution(17891927789715655548)
XLA Ops:
  6.6 0.1 all-gather.3.cloned.1.call-start
  6.6 1.0 copy.40
  7.6 0.1 broadcast_in_dim.16
  7.7 47.2 %all_to_all.38 = bf16[16,128,128]{1,2,0:T(8,128)(2,1)} all-to-all(bf16[16,128,128]{1,2,0:T(8,128)(2,1)S(1)} %broadcast_in_dim.16), channel_id=1, replica_groups=mesh['grp'=2,'sp'=16,'tp'=8] {'sp'}, dimensions={0} | all-to-all | bytes 1048576 | tf_op jit(solution)/shard_map/all_to_all | solution.py:20
  54.9 0.1 all-gather.3.cloned.1.call-update
  54.9 0.1 all-gather.5.cloned.1.call-start
  55.0 1.1 copy.41
  56.1 1.1 copy.42
  57.2 0.0 copy-start.8
  57.2 1.8 pad_maximum_fusion
  59.0 0.1 all-gather.5.cloned.1.call-update
  59.1 5.3 %collective-permute-start.1 = (s32[128]{0:T(128)S(1)}, s32[128]{0:T(128)S(1)}, u32[]{:S(2)}, u32[]{:S(2)}) collective-permute-start(s32[128]{0:T(128)S(1)} %slice.49), channel_id=1, source_target_pairs={{0,8},{8,16},{16,24},{24,32},{32,40},{40,48},{48,56},{56,64},{64,7... | collective-permute-start | bytes 1544 | tf_op jit(solution)/shard_map/ppermute | solution.py:15
  64.4 2.2 collective-permute-start
  66.6 4.6 %collective-permute-start.2 = (bf16[128,64]{0,1:T(8,128)(2,1)S(1)}, bf16[128,64]{0,1:T(8,128)(2,1)S(1)}, u32[]{:S(2)}, u32[]{:S(2)}) collective-permute-start(bf16[128,64]{0,1:T(8,128)(2,1)S(1)} %slice.52), channel_id=1, source_target_pairs={{0,8},{8,16},{16,24},{24,32},{32,40},{40,48},{48,56},{56,64},{64,7... | collective-permute-start | bytes 49160 | tf_op jit(solution)/shard_map/ppermute | solution.py:15
  71.3 0.2 reshape.172
  71.5 0.0 collective-permute-done.1
  71.6 1.0 fusion.30
  72.6 0.5 fusion.48
  73.1 0.1 broadcast_maximum_fusion
  73.2 0.2 fusion.7
  73.4 0.1 fusion.43
  73.5 0.4 fusion.13
  73.9 0.4 copy.48
  74.3 0.0 copy-start.3
  74.3 0.0 copy-start.6
  74.3 0.2 reshape.173
  74.5 18.0 %all_to_all.39 = bf16[8,96,128]{2,1,0:T(8,128)(2,1)S(1)} all-to-all(bf16[8,96,128]{2,1,0:T(8,128)(2,1)S(1)} %reshape.173), channel_id=1, replica_groups=mesh['grp'=2,'sp'=16,'tp'=8] {'tp'}, dimensions={0} | all-to-all | bytes 393216 | tf_op jit(solution)/shard_map/all_to_all | solution.py:133
  92.5 9.6 %all-gather.3.cloned.1.call-done = bf16[1024,2048]{0,1:T(8,128)(2,1)} async-done(((bf16[128,2048]{0,1:T(8,128)(2,1)}), bf16[1024,2048]{0,1:T(8,128)(2,1)}) %all-gather.3.cloned.1.call-update) | async-done | bytes 4194320 | tf_op jit(solution)/shard_map/all_gather | solution.py:136
  102.0 3.6 %convolution_convert_fusion.1 = bf16[96,2048]{1,0:T(8,128)(2,1)S(1)} fusion(bf16[1024,2048]{0,1:T(8,128)(2,1)} %all-gather.3.cloned.1.call-done, bf16[8,96,128]{2,1,0:T(8,128)(2,1)S(1)} %all_to_all.39), kind=kOutput, calls=%fused_computation.7 | convolution fusion | flops 402849792 | bytes 4784128 | tf_op jit(solution)/shard_map/dot_general | solution.py:134
  105.7 0.2 fusion.14
  105.8 0.2 fusion.17
  106.1 0.2 fusion.21
  106.3 0.2 constant_dynamic-update-slice_fusion.7
  106.4 0.2 constant_dynamic-update-slice_fusion.6
  106.6 0.2 constant_dynamic-update-slice_fusion.5
  106.8 0.2 constant_dynamic-update-slice_fusion.4
  106.9 0.2 constant_dynamic-update-slice_fusion.3
  107.1 0.2 constant_dynamic-update-slice_fusion.2
  107.2 0.2 constant_dynamic-update-slice_fusion.1
  107.4 0.2 constant_dynamic-update-slice_fusion
  107.6 41.4 %all_to_all.40 = bf16[8,96,2048]{2,1,0:T(8,128)(2,1)S(1)} all-to-all(bf16[8,96,2048]{2,1,0:T(8,128)(2,1)S(1)} %bitcast.86), channel_id=1, replica_groups=mesh['grp'=2,'sp'=16,'tp'=8] {'tp'}, dimensions={0} | all-to-all | bytes 6291456 | tf_op jit(solution)/shard_map/all_to_all | solution.py:149
  149.0 82.2 %all-gather.5.cloned.1.call-done = bf16[2048,2304]{0,1:T(8,128)(2,1)} async-done(((bf16[128,2304]{0,1:T(8,128)(2,1)}), bf16[2048,2304]{0,1:T(8,128)(2,1)}) %all-gather.5.cloned.1.call-update) | async-done | bytes 9437200 | tf_op jit(solution)/shard_map/all_gather | solution.py:39
  231.2 6.0 %fusion.3 = f32[768,768]{1,0:T(8,128)} fusion(bf16[768,2048]{1,0:T(8,128)(2,1)S(1)} %bitcast.87, bf16[2048,2304]{0,1:T(8,128)(2,1)} %all-gather.5.cloned.1.call-done), kind=kOutput, calls=%fused_computation.4 | convolution fusion | flops 2415919104 | bytes 8650752 | tf_op jit(solution)/shard_map/dot_general | solution.py:150
  237.1 11.0 %convolution_convert_fusion = bf16[768,2048]{1,0:T(8,128)(2,1)} fusion(bf16[2048,2304]{0,1:T(8,128)(2,1)} %all-gather.5.cloned.1.call-done, f32[768,768]{1,0:T(8,128)} %fusion.3, bf16[768,2048]{1,0:T(8,128)(2,1)S(1)} %bitcast.88), kind=kOutput, calls=%fused_computation | convolution fusion | flops 4836950016 | bytes 14942208 | tf_op jit(solution)/shard_map/dot_general | solution.py:155
  248.1 51.4 %all_to_all.41 = bf16[8,96,2048]{2,1,0:T(8,128)(2,1)S(1)} all-to-all(bf16[8,96,2048]{2,1,0:T(8,128)(2,1)} %bitcast.89), channel_id=1, replica_groups=mesh['grp'=2,'sp'=16,'tp'=8] {'tp'}, dimensions={0} | all-to-all | bytes 6291456 | tf_op jit(solution)/shard_map/all_to_all | solution.py:55
  299.5 1.4 reduce_sum.54
  300.9 1.2 fusion.18
  302.1 2.0 fusion.24
  (34 shorter events, 0.2 us)
Async XLA Ops:
  6.5 52.5 %copy-start.5 = (s32[768]{0:T(1024)S(1)}, s32[768]{0:T(1024)}, u32[]{:S(2)}) copy-start(s32[768]{0:T(1024)} %param.16) | copy-start | bytes 9220
  6.5 57.8 %copy-start.2 = (bf16[768,64]{0,1:T(8,128)(2,1)S(1)}, bf16[768,64]{0,1:T(8,128)(2,1)}, u32[]{:S(2)}) copy-start(bf16[768,64]{0,1:T(8,128)(2,1)} %param.15) | copy-start | bytes 294916
  6.6 60.1 %copy-start.1 = (bf16[768,64]{0,1:T(8,128)(2,1)S(1)}, bf16[768,64]{0,1:T(8,128)(2,1)}, u32[]{:S(2)}) copy-start(bf16[768,64]{0,1:T(8,128)(2,1)} %param.14) | copy-start | bytes 294916
  6.6 64.8 %copy-start.4 = (bf16[768,128]{1,0:T(8,128)(2,1)S(1)}, bf16[768,128]{1,0:T(8,128)(2,1)}, u32[]{:S(2)}) copy-start(bf16[768,128]{1,0:T(8,128)(2,1)} %param.13) | copy-start | bytes 589828
  6.6 95.5 %all-gather.3.cloned.1.call-start = ((), (), s32[]{:S(2)}) async-start(), calls=%async_computation.4 | async-start | bytes 4718592 | tf_op jit(solution)/shard_map/all_gather | solution.py:136
  54.9 176.2 %all-gather.5.cloned.1.call-start = ((), (), s32[]{:S(2)}) async-start(), calls=%async_computation.5 | async-start | bytes 10027008 | tf_op jit(solution)/shard_map/all_gather | solution.py:39
  57.2 15.9 %copy-start.8 = (f32[2]{0:T(128)S(1)}, f32[2]{0:T(128)}, u32[]{:S(2)}) copy-start(f32[2]{0:T(128)} %param.17) | copy-start | bytes 28
  59.1 12.4 %collective-permute-start.1 = (s32[128]{0:T(128)S(1)}, s32[128]{0:T(128)S(1)}, u32[]{:S(2)}, u32[]{:S(2)}) collective-permute-start(s32[128]{0:T(128)S(1)} %slice.49), channel_id=1, source_target_pairs={{0,8},{8,16},{16,24},{24,32},{32,40},{40,48},{48,56},{56,64},{64,7... | collective-permute-start | bytes 1544 | tf_op jit(solution)/shard_map/ppermute | solution.py:15
  64.4 8.2 %collective-permute-start = (bf16[128,64]{0,1:T(8,128)(2,1)S(1)}, bf16[128,64]{0,1:T(8,128)(2,1)S(1)}, u32[]{:S(2)}, u32[]{:S(2)}) collective-permute-start(bf16[128,64]{0,1:T(8,128)(2,1)S(1)} %slice.45), channel_id=1, source_target_pairs={{0,8},{8,16},{16,24},{24,32},{32,40},{40,48},{48,56},{56,64},{64,7... | collective-permute-start | bytes 49160 | tf_op jit(solution)/shard_map/ppermute | solution.py:15
  66.6 5.9 %collective-permute-start.2 = (bf16[128,64]{0,1:T(8,128)(2,1)S(1)}, bf16[128,64]{0,1:T(8,128)(2,1)S(1)}, u32[]{:S(2)}, u32[]{:S(2)}) collective-permute-start(bf16[128,64]{0,1:T(8,128)(2,1)S(1)} %slice.52), channel_id=1, source_target_pairs={{0,8},{8,16},{16,24},{24,32},{32,40},{40,48},{48,56},{56,64},{64,7... | collective-permute-start | bytes 49160 | tf_op jit(solution)/shard_map/ppermute | solution.py:15
  74.3 31.6 %copy-start.3 = (bf16[96,2048]{1,0:T(8,128)(2,1)S(1)}, bf16[96,2048]{1,0:T(8,128)(2,1)}, u32[]{:S(2)}) copy-start(bf16[96,2048]{1,0:T(8,128)(2,1)} %param.19) | copy-start | bytes 1179652
  74.3 31.6 %copy-start.6 = (f32[2048]{0:T(1024)S(1)}, f32[2048]{0:T(1024)}, u32[]{:S(2)}) copy-start(f32[2048]{0:T(1024)} %param.20) | copy-start | bytes 24580
  92.5 13.8 %copy-start = (f32[2048]{0:T(1024)S(1)}, f32[2048]{0:T(1024)}, u32[]{:S(2)}) copy-start(f32[2048]{0:T(1024)} %param.21) | copy-start | bytes 24580
  299.5 2.6 copy-start.7
Sparse Core Ops, SparseCore 0:
  55.1 46.9 all-gather.2
  103.8 127.3 all-gather.4
